TPU v7x, 32 devices: a whole 2x2x4 slice. The times are simulated.
32 devices in a mesh: kv: 16 (over z, y, core), tp: 2 (over x).
Axes of the slice: x: 2, y: 2, z: 4, core: 2. Of those that a mesh axis runs over, the one named last changes fastest.
Arguments:
- queries: bfloat16 [4096, 4, 128], P('kv', 'tp'), may hold values from -6 to 6
- keys: bfloat16 [4096, 4, 128], P('kv', 'tp'), may hold values from -6 to 6
- values: bfloat16 [4096, 4, 128], P('kv', 'tp'), may hold values from -6 to 6
- attended: bfloat16 [4096, 4, 128], P('kv', 'tp'), may hold values from -6 to 6
- out_grad: bfloat16 [4096, 4, 128], P('kv', 'tp'), may hold values from -6 to 6
- log_sum: float32 [4096, 4], P('kv', 'tp'), may hold values from 2.5 to 4.5
- picked: int32 [32, 16], P('kv'), may hold values from -1 to 127, as said below
- layer_input: bfloat16 [4096, 4096], P('kv'), may hold values from -0.03125 to 0.03125
Outputs:
- query_grad: float32 [4096, 4, 128], P('kv', 'tp')
- key_grad: float32 [4096, 4, 128], P('kv', 'tp')
- value_grad: float32 [4096, 4, 128], P('kv', 'tp')
- weight_grad: float32 [4096, 512], P('kv', 'tp')
Inputs may be any that keep to these rules, and one draw needn't show every extreme that they name: Row r lists distinct key block numbers picked by query block r, followed by -1 to the end of the row; at least one entry is not -1, and at most 16 are. No picked block starts after the last position of its query block. With the span of a position being the position divided by 256 (rounded down), the span of every picked block is the query block's span or that span less 1, 2, 4, 8 and so on. The query blocks of one span pick at most 4 distinct blocks from any other single span.
All inputs are finite; a program needn't handle non-finite values.
Results may differ from a plain program's by a relative error of at most 0.004.
Values may be sent and summed in bfloat16 or wider, within the bound.
A program may use at most 64 MiB of HBM per device.

v0:
```python
import functools

import jax
import jax.numpy as jnp
from jax import lax
from jax.experimental import pallas as pl
from jax.experimental.pallas import tpu as pltpu
from jax.sharding import PartitionSpec as P

QB = 128
KB = 32
PER_SPAN = 4
COMPACT = PER_SPAN * KB
CHUNKS = 8
F32 = jnp.float32
BF16 = jnp.bfloat16


def xor(value, bits):
    out = value
    for i in range(bits.bit_length()):
        if bits >> i & 1:
            out = out + (1 << i) - (2 << i) * lax.rem(value // (1 << i), 2)
    return out


def dot_nt(a, b):
    return lax.dot_general(a, b, (((1,), (1,)), ((), ())), preferred_element_type=F32)


def dot_tn(a, b):
    return lax.dot_general(a, b, (((0,), (0,)), ((), ())), preferred_element_type=F32)


def dot_nn(a, b):
    return lax.dot_general(a, b, (((1,), (0,)), ((), ())), preferred_element_type=F32)


def body(
    n, levels, heads, dh,
    picked, q, k, v, att, og, log_sum, x_hbm,
    dq_out, dk_out, dv_out, wg_out,
    x, slot, slot_in, pick, ksend, kin, vsend, vin, dvsend, dvin, dksend, dkin,
    wts, part, got1, send2, got2, send3, got3,
    x_sem, slot_ss, slot_rs, k_ss, k_rs, v_ss, v_rs, dv_ss, dv_rs, dk_ss, dk_rs,
    s1_ss, s1_rs, s2_ss, s2_rs, s3_ss, s3_rs,
):
    me = lax.axis_index("kv")
    tok, cols = q.shape
    query_count = tok // QB
    span_blocks = tok // KB
    rows = slot.shape[0]
    scale = dh ** (-0.5)
    quarter = n // 4
    rb = wg_out.shape[0]
    order = list(reversed(range(levels)))

    def to(offset):
        return {"kv": lax.rem(me + offset + n, n)}

    def flipped(bits):
        low = lax.rem(me, 4)
        high = me // 4
        if bits == 1:
            return {"kv": me + 1 - 2 * lax.rem(me, 2)}
        if bits == 2:
            return {"kv": me + 2 - 4 * (low // 2)}
        return {"kv": xor(high, bits // 4) * 4 + low}

    def remote(src, dst, ss, rs, device):
        return pltpu.make_async_remote_copy(
            src_ref=src, dst_ref=dst, send_sem=ss, recv_sem=rs,
            device_id=device, device_id_type=pl.DeviceIdType.MESH,
        )

    load_x = pltpu.make_async_copy(x_hbm, x, x_sem)
    load_x.start()
    barrier = pltpu.get_barrier_semaphore()
    greeted = [to(1 << l) for l in range(levels)] + [to(-(1 << l)) for l in range(levels)]
    greeted += [flipped(1), flipped(2)] + [flipped(4 * b) for b in range(1, quarter)]
    for device in greeted:
        pl.semaphore_signal(
            barrier, inc=1, device_id=device, device_id_type=pl.DeviceIdType.MESH
        )

    row = lax.broadcasted_iota(jnp.int32, (rows, tok), 0)
    lane = lax.broadcasted_iota(jnp.int32, (rows, tok), 1)
    back = jnp.zeros((rows, tok), jnp.int32)
    for l in range(levels):
        back = jnp.where(row == l + 1, 1 << l, back)
    ids = jnp.where(row <= levels, (me - back) * span_blocks + lane // KB, -2)
    live = []
    for b in range(query_count):
        hit = jnp.zeros((rows, tok), jnp.int32)
        for s in range(picked.shape[1]):
            p = picked[b, s]
            hit = jnp.where(ids == jnp.where(p < 0, -(1 << 30), p), 1, hit)
        live.append(hit.astype(F32))
    need = functools.reduce(jnp.maximum, live)
    below = lax.broadcasted_iota(jnp.int32, (tok, tok), 0)
    above = lax.broadcasted_iota(jnp.int32, (tok, tok), 1)
    steps = jnp.where((below % KB == 0) & (below // KB < above // KB), 1.0, 0.0).astype(BF16)
    rank = dot_nn(need.astype(BF16), steps)
    slot[...] = jnp.where(need > 0, rank * KB + (lane % KB).astype(F32), -1.0)

    pl.semaphore_wait(barrier, len(greeted))
    slot_copies = {}
    for l in order:
        slot_copies[l] = remote(
            slot, slot_in.at[l], slot_ss.at[l], slot_rs.at[l], to(-(1 << l))
        )
        slot_copies[l].start()

    def one_hot(row_values):
        sub = lax.broadcasted_iota(jnp.int32, (COMPACT, tok), 0).astype(F32)
        return jnp.where(sub == row_values, 1.0, 0.0).astype(BF16)

    head = [slice(h * dh, (h + 1) * dh) for h in range(heads)]
    k_copies, v_copies = {}, {}
    for l in order:
        slot_copies[l].wait_recv()
        chosen = one_hot(slot_in[l, l + 1 : l + 2, :])
        pick[l] = chosen
        ksend[l] = dot_nn(chosen, k[...]).astype(BF16)
        k_copies[l] = remote(ksend.at[l], kin.at[l], k_ss.at[l], k_rs.at[l], to(1 << l))
        k_copies[l].start()
    for l in order:
        vsend[l] = dot_nn(pick[l], v[...]).astype(BF16)
        v_copies[l] = remote(vsend.at[l], vin.at[l], v_ss.at[l], v_rs.at[l], to(1 << l))
        v_copies[l].start()

    dots = [
        jnp.sum(og[:, c].astype(F32) * att[:, c].astype(F32), axis=1, keepdims=True) for c in head
    ]
    stored = [log_sum[:, h : h + 1] for h in range(heads)]

    def spread(pieces):
        return jnp.concatenate(
            [jnp.broadcast_to(p, (QB, p.shape[1])) for p in pieces], axis=0
        )

    own_live = spread([m[0:1, :] for m in live]) > 0
    own_live = own_live & (above <= below)
    for h, c in enumerate(head):
        w = jnp.where(own_live, jnp.exp(dot_nt(q[:, c], k[:, c]) * scale - stored[h]), 0.0)
        dv_out[:, c] = dot_tn(w.astype(BF16), og[:, c])
        g = (w * (dot_nt(og[:, c], v[:, c]) - dots[h])).astype(BF16)
        dq_out[:, c] = dot_nn(g, k[:, c])
        dk_out[:, c] = dot_tn(g, q[:, c])

    dv_copies, dk_copies = {}, {}
    for l in order:
        mine = one_hot(slot[l + 1 : l + 2, :])
        mask = spread([dot_nt(m.astype(BF16), mine)[l + 1 : l + 2, :] for m in live]) > 0
        k_copies[l].wait_recv()
        for h, c in enumerate(head):
            w = jnp.where(mask, jnp.exp(dot_nt(q[:, c], kin[l, :, c]) * scale - stored[h]), 0.0)
            wts[l, h] = w
            dvsend[l, :, c] = dot_tn(w.astype(BF16), og[:, c]).astype(BF16)
        dv_copies[l] = remote(
            dvsend.at[l], dvin.at[l], dv_ss.at[l], dv_rs.at[l], to(-(1 << l))
        )
        dv_copies[l].start()
    for l in order:
        v_copies[l].wait_recv()
        for h, c in enumerate(head):
            g = (wts[l, h] * (dot_nt(og[:, c], vin[l, :, c]) - dots[h])).astype(BF16)
            dq_out[:, c] += dot_nn(g, kin[l, :, c])
            dksend[l, :, c] = (dot_tn(g, q[:, c]) * scale).astype(BF16)
        dk_copies[l] = remote(
            dksend.at[l], dkin.at[l], dk_ss.at[l], dk_rs.at[l], to(-(1 << l))
        )
        dk_copies[l].start()
    dq_out[...] = dq_out[...] * scale

    total = dv_out[...]
    for l in order:
        dv_copies[l].wait_recv()
        total += dot_tn(pick[l], dvin[l])
    dv_out[...] = total
    rounded = total.astype(BF16)
    load_x.wait()
    core = lax.rem(me, 2)
    per = (n // 2) // CHUNKS
    width = x.shape[1] // CHUNKS
    s1 = []
    for i in range(CHUNKS):
        w = dot_tn(x[:, i * width : (i + 1) * width], rounded).reshape(per, 2, rb, cols)
        part[0, i * per : (i + 1) * per] = w[:, 0]
        part[1, i * per : (i + 1) * per] = w[:, 1]
        copy = remote(
            part.at[1 - core, pl.ds(i * per, per)], got1.at[pl.ds(i * per, per)],
            s1_ss.at[i], s1_rs.at[i], flipped(1),
        )
        copy.start()
        s1.append(copy)
    for copy in s1:
        copy.wait()
    up = lax.rem(me, 4) // 2
    high = me // 4
    s2, s3 = [], []
    for b in reversed(range(quarter)):
        at = 2 * xor(high, b) + 1 - up
        send2[b] = (part[core, at] + got1[at]).astype(BF16)
        copy = remote(send2.at[b], got2.at[b], s2_ss.at[b], s2_rs.at[b], flipped(2))
        copy.start()
        s2.append(copy)
    for b, copy in zip(reversed(range(quarter)), s2):
        at = 2 * xor(high, b) + up
        kept = part[core, at] + got1[at]
        copy.wait_recv()
        kept = kept + got2[b].astype(F32)
        if b == 0:
            wg_out[...] = kept
        else:
            send3[b] = kept.astype(BF16)
            copy = remote(send3.at[b], got3.at[b], s3_ss.at[b], s3_rs.at[b], flipped(4 * b))
            copy.start()
            s3.append(copy)

    total = dk_out[...] * scale
    for l in order:
        dk_copies[l].wait_recv()
        total += dot_tn(pick[l], dkin[l])
    dk_out[...] = total

    for b, copy in zip(reversed(range(1, quarter)), s3):
        copy.wait_recv()
        wg_out[...] += got3[b].astype(F32)
    for copies in (slot_copies, k_copies, v_copies, dv_copies, dk_copies):
        for l in order:
            copies[l].wait_send()
    for copy in s2 + s3:
        copy.wait_send()


def per_device(queries, keys, values, attended, out_grad, log_sum, picked, layer_input):
    tok, heads, dh = queries.shape
    n = lax.axis_size("kv")
    levels = n.bit_length() - 1
    cols = heads * dh
    width = layer_input.shape[1]
    rb = width // n
    rows = (levels + 1 + 7) // 8 * 8
    flat = [a.reshape(tok, cols) for a in (queries, keys, values, attended, out_grad)]
    vmem = pl.BlockSpec(memory_space=pltpu.VMEM)
    sems = pltpu.SemaphoreType.DMA
    level_buf = pltpu.VMEM((levels, COMPACT, cols), BF16)
    out = pl.pallas_call(
        functools.partial(body, n, levels, heads, dh),
        out_shape=[jax.ShapeDtypeStruct((tok, cols), F32)] * 3
        + [jax.ShapeDtypeStruct((rb, cols), F32)],
        in_specs=[pl.BlockSpec(memory_space=pltpu.SMEM)] + [vmem] * 6
        + [pl.BlockSpec(memory_space=pl.ANY)],
        out_specs=[vmem] * 4,
        scratch_shapes=[
            pltpu.VMEM((tok, width), BF16),
            pltpu.VMEM((rows, tok), F32),
            pltpu.VMEM((levels, rows, tok), F32),
            pltpu.VMEM((levels, COMPACT, tok), BF16),
        ]
        + [level_buf] * 8
        + [
            pltpu.VMEM((levels, heads, tok, COMPACT), F32),
            pltpu.VMEM((2, n // 2, rb, cols), F32),
            pltpu.VMEM((n // 2, rb, cols), F32),
            pltpu.VMEM((n // 4, rb, cols), BF16),
            pltpu.VMEM((n // 4, rb, cols), BF16),
            pltpu.VMEM((n // 4, rb, cols), BF16),
            pltpu.VMEM((n // 4, rb, cols), BF16),
            sems,
        ]
        + [sems((levels,))] * 10
        + [sems((CHUNKS,))] * 2
        + [sems((n // 4,))] * 4,
        compiler_params=pltpu.CompilerParams(
            collective_id=0, has_side_effects=True, vmem_limit_bytes=48 * 1024 * 1024
        ),
    )(picked, *flat, log_sum, layer_input)
    grads = [g.reshape(tok, heads, dh) for g in out[:3]]
    return (*grads, out[3])


def solution(mesh):
    placed = (P("kv", "tp", None),) * 5 + (P("kv", "tp"), P("kv", None), P("kv", None))
    return jax.shard_map(
        per_device,
        mesh=mesh,
        in_specs=placed,
        out_specs=(P("kv", "tp", None), P("kv", "tp", None), P("kv", "tp", None), P("kv", "tp")),
        check_vma=False,
    )
```

profile of v0, /device:TPU:0, one launch (start us, length us, event | category | flops | bytes accessed | tf_op | source)
XLA Modules:
  0.0 62.2 jit_solution(7654114996690926454)
XLA Ops:
  0.6 0.9 %copy.23 = bf16[32,8,2,128]{3,1,2,0:T(8,128)(2,1)S(1)} copy(bf16[32,8,2,128]{3,2,1,0:T(2,128)(2,1)} %bitcast.17) | data formatting | bytes 262144
  1.6 0.8 %copy.12.log_sum = f32[256,2]{1,0:T(8,128)S(1)} copy(f32[256,2]{0,1:T(2,128)} %param.13) | data formatting | bytes 4096 | tf_op args[5]
  2.4 1.0 %copy_bitcast_fusion.2 = (bf16[256,256]{1,0:T(8,128)(2,1)S(1)}, bf16[256,256]{1,0:T(8,128)(2,1)S(1)}) fusion(bf16[32,8,2,128]{3,2,1,0:T(2,128)(2,1)} %bitcast.18, bf16[32,8,2,128]{3,2,1,0:T(2,128)(2,1)} %bitcast.19), kind=kLoop, calls=%fused_computation.2 | loop fusion | bytes 524288 | tf_op jit(solution)/shard_map/reshape | solution.py:245
  3.4 1.0 %copy_bitcast_fusion = (bf16[256,256]{1,0:T(8,128)(2,1)S(1)}, bf16[256,256]{1,0:T(8,128)(2,1)S(1)}) fusion(bf16[32,8,2,128]{3,2,1,0:T(2,128)(2,1)} %bitcast.20, bf16[32,8,2,128]{3,2,1,0:T(2,128)(2,1)} %bitcast.21), kind=kLoop, calls=%fused_computation | loop fusion | bytes 524288 | tf_op jit(solution)/shard_map/reshape | solution.py:245
  4.4 0.0 copy-start
  4.4 1.6 %copy-done = bf16[256,4096]{1,0:T(8,128)(2,1)S(1)} copy-done((bf16[256,4096]{1,0:T(8,128)(2,1)S(1)}, bf16[256,4096]{1,0:T(8,128)(2,1)}, u32[]{:S(2)}) %copy-start) | copy-done | bytes 2097176
  6.0 0.0 copy-start.1
  6.0 0.7 %copy-done.1 = s32[2,16]{1,0:T(2,128)S(1)} copy-done((s32[2,16]{1,0:T(2,128)S(1)}, s32[2,16]{1,0:T(2,128)}, u32[]{:S(2)}) %copy-start.1) | copy-done | bytes 152
  6.7 52.3 %shard_map.111 = (f32[256,256]{1,0:T(8,128)S(1)}, f32[256,256]{1,0:T(8,128)S(1)}, f32[256,256]{1,0:T(8,128)S(1)}, f32[256,256]{1,0:T(8,128)S(1)}) custom-call(s32[2,16]{1,0:T(2,128)S(1)} %copy-done.1, bf16[256,256]{1,0:T(8,128)(2,1)S(1)} %bitcast.16, bf16[256,256]{1,0:T(8,128)(2,1)S(1)} %get-tuple-element.15.k, bf16[256,256]{1,0:T(8,128)(2,1)S(1)} %get-tuple-element.14.v, ...), custom_call_target="tpu_custom_call" | custom-call | tf_op jit(solution)/shard_map/pallas_call | solution.py:249
  59.0 0.8 %reshape.37 = f32[256,2,128]{2,1,0:T(2,128)} reshape(f32[256,256]{1,0:T(8,128)S(1)} %get-tuple-element.8) | data formatting | bytes 524288 | tf_op jit(solution)/shard_map/reshape | solution.py:280
  59.8 0.8 %reshape.38 = f32[256,2,128]{2,1,0:T(2,128)} reshape(f32[256,256]{1,0:T(8,128)S(1)} %get-tuple-element.9) | data formatting | bytes 524288 | tf_op jit(solution)/shard_map/reshape | solution.py:280
  60.7 0.8 %reshape.39 = f32[256,2,128]{2,1,0:T(2,128)} reshape(f32[256,256]{1,0:T(8,128)S(1)} %get-tuple-element.10) | data formatting | bytes 524288 | tf_op jit(solution)/shard_map/reshape | solution.py:280
  61.5 0.7 %copy.25 = f32[256,256]{1,0:T(8,128)} copy(f32[256,256]{1,0:T(8,128)S(1)} %get-tuple-element.23) | data formatting | bytes 524288
Async XLA Ops:
  4.4 1.6 %copy-start = (bf16[256,4096]{1,0:T(8,128)(2,1)S(1)}, bf16[256,4096]{1,0:T(8,128)(2,1)}, u32[]{:S(2)}) copy-start(bf16[256,4096]{1,0:T(8,128)(2,1)} %x_hbm.1) | copy-start | bytes 6291460
  6.0 0.7 %copy-start.1 = (s32[2,16]{1,0:T(2,128)S(1)}, s32[2,16]{1,0:T(2,128)}, u32[]{:S(2)}) copy-start(s32[2,16]{1,0:T(2,128)} %picked.1) | copy-start | bytes 388
where the time goes:
time: 62.4 us; the launch traced here: 62.2 us
  Pallas kernels  52.3 us (84%)
  local copies, waits for them, and re-layouts  9.21 us (15%)
  between operations  0.67 us (1%)
    pallas_call x1, Pallas kernels, per_device(): pl.pallas_call(functools.partial(body, n, levels, heads, dh), out_shape=[...  52.3 us
    unnamed x7, local copies, waits for them, and re-layouts  4.7 us
    reshape x3, local copies, waits for them, and re-layouts, per_device(): grads = [g.reshape(tok, heads, dh) for g in out[:3]]  2.5 us
    reshape x2, local copies, waits for them, and re-layouts, per_device(): a.reshape(tok, cols)  2.01 us

commit v1 on v0

--- a/solution.py
+++ b/solution.py
@@ -38,11 +38,11 @@
 
 def body(
     n, levels, heads, dh,
-    picked, q, k, v, att, og, log_sum, x_hbm,
+    picked_hbm, q_hbm, k_hbm, v_hbm, att_hbm, og_hbm, log_sum, x_hbm,
     dq_out, dk_out, dv_out, wg_out,
-    x, slot, slot_in, pick, ksend, kin, vsend, vin, dvsend, dvin, dksend, dkin,
+    picked, raw, q, k, v, att, og, x, xt, slot, slot_in, pick, ksend, kin, vsend, vin, dvsend, dvin, dksend, dkin,
     wts, part, got1, send2, got2, send3, got3,
-    x_sem, slot_ss, slot_rs, k_ss, k_rs, v_ss, v_rs, dv_ss, dv_rs, dk_ss, dk_rs,
+    x_sem, picked_sem, raw_sem, slot_ss, slot_rs, k_ss, k_rs, v_ss, v_rs, dv_ss, dv_rs, dk_ss, dk_rs,
     s1_ss, s1_rs, s2_ss, s2_rs, s3_ss, s3_rs,
 ):
     me = lax.axis_index("kv")
@@ -73,6 +73,21 @@
             device_id=device, device_id_type=pl.DeviceIdType.MESH,
         )
 
+    load_picked = pltpu.make_async_copy(picked_hbm, picked, picked_sem)
+    load_picked.start()
+    loads = {}
+    for i, (src, dst) in enumerate(
+        ((k_hbm, k), (v_hbm, v), (q_hbm, q), (og_hbm, og), (att_hbm, att))
+    ):
+        loads[i] = (pltpu.make_async_copy(src, raw.at[i], raw_sem.at[i]), dst)
+        loads[i][0].start()
+
+    def settle(i):
+        copy, dst = loads[i]
+        copy.wait()
+        for h in range(heads):
+            dst[:, h * dh : (h + 1) * dh] = raw[i, :, h, :]
+
     load_x = pltpu.make_async_copy(x_hbm, x, x_sem)
     load_x.start()
     barrier = pltpu.get_barrier_semaphore()
@@ -89,6 +104,7 @@
     for l in range(levels):
         back = jnp.where(row == l + 1, 1 << l, back)
     ids = jnp.where(row <= levels, (me - back) * span_blocks + lane // KB, -2)
+    load_picked.wait()
     live = []
     for b in range(query_count):
         hit = jnp.zeros((rows, tok), jnp.int32)
@@ -103,89 +119,124 @@
     rank = dot_nn(need.astype(BF16), steps)
     slot[...] = jnp.where(need > 0, rank * KB + (lane % KB).astype(F32), -1.0)
 
+    settle(0)
+    settle(1)
     pl.semaphore_wait(barrier, len(greeted))
+
+    def sends_up(l):
+        return me + (1 << l) < n
+
+    def sends_down(l):
+        return me >= 1 << l
+
     slot_copies = {}
     for l in order:
         slot_copies[l] = remote(
             slot, slot_in.at[l], slot_ss.at[l], slot_rs.at[l], to(-(1 << l))
         )
-        slot_copies[l].start()
+        pl.when(sends_down(l))(slot_copies[l].start)
 
     def one_hot(row_values):
         sub = lax.broadcasted_iota(jnp.int32, (COMPACT, tok), 0).astype(F32)
         return jnp.where(sub == row_values, 1.0, 0.0).astype(BF16)
 
     head = [slice(h * dh, (h + 1) * dh) for h in range(heads)]
-    k_copies, v_copies = {}, {}
-    for l in order:
-        slot_copies[l].wait_recv()
-        chosen = one_hot(slot_in[l, l + 1 : l + 2, :])
-        pick[l] = chosen
-        ksend[l] = dot_nn(chosen, k[...]).astype(BF16)
+    k_copies, v_copies, dv_copies, dk_copies = {}, {}, {}, {}
+    for l in order:
         k_copies[l] = remote(ksend.at[l], kin.at[l], k_ss.at[l], k_rs.at[l], to(1 << l))
-        k_copies[l].start()
-    for l in order:
-        vsend[l] = dot_nn(pick[l], v[...]).astype(BF16)
         v_copies[l] = remote(vsend.at[l], vin.at[l], v_ss.at[l], v_rs.at[l], to(1 << l))
-        v_copies[l].start()
-
-    dots = [
-        jnp.sum(og[:, c].astype(F32) * att[:, c].astype(F32), axis=1, keepdims=True) for c in head
-    ]
-    stored = [log_sum[:, h : h + 1] for h in range(heads)]
-
-    def spread(pieces):
-        return jnp.concatenate(
-            [jnp.broadcast_to(p, (QB, p.shape[1])) for p in pieces], axis=0
-        )
-
-    own_live = spread([m[0:1, :] for m in live]) > 0
-    own_live = own_live & (above <= below)
-    for h, c in enumerate(head):
-        w = jnp.where(own_live, jnp.exp(dot_nt(q[:, c], k[:, c]) * scale - stored[h]), 0.0)
-        dv_out[:, c] = dot_tn(w.astype(BF16), og[:, c])
-        g = (w * (dot_nt(og[:, c], v[:, c]) - dots[h])).astype(BF16)
-        dq_out[:, c] = dot_nn(g, k[:, c])
-        dk_out[:, c] = dot_tn(g, q[:, c])
-
-    dv_copies, dk_copies = {}, {}
-    for l in order:
-        mine = one_hot(slot[l + 1 : l + 2, :])
-        mask = spread([dot_nt(m.astype(BF16), mine)[l + 1 : l + 2, :] for m in live]) > 0
-        k_copies[l].wait_recv()
-        for h, c in enumerate(head):
-            w = jnp.where(mask, jnp.exp(dot_nt(q[:, c], kin[l, :, c]) * scale - stored[h]), 0.0)
-            wts[l, h] = w
-            dvsend[l, :, c] = dot_tn(w.astype(BF16), og[:, c]).astype(BF16)
         dv_copies[l] = remote(
             dvsend.at[l], dvin.at[l], dv_ss.at[l], dv_rs.at[l], to(-(1 << l))
         )
-        dv_copies[l].start()
-    for l in order:
-        v_copies[l].wait_recv()
-        for h, c in enumerate(head):
-            g = (wts[l, h] * (dot_nt(og[:, c], vin[l, :, c]) - dots[h])).astype(BF16)
-            dq_out[:, c] += dot_nn(g, kin[l, :, c])
-            dksend[l, :, c] = (dot_tn(g, q[:, c]) * scale).astype(BF16)
         dk_copies[l] = remote(
             dksend.at[l], dkin.at[l], dk_ss.at[l], dk_rs.at[l], to(-(1 << l))
         )
-        dk_copies[l].start()
+    for l in order:
+
+        @pl.when(sends_up(l))
+        def _(l=l):
+            slot_copies[l].wait_recv()
+            chosen = one_hot(slot_in[l, l + 1 : l + 2, :])
+            pick[l] = chosen
+            ksend[l] = dot_nn(chosen, k[...]).astype(BF16)
+            k_copies[l].start()
+
+    for l in order:
+
+        @pl.when(sends_up(l))
+        def _(l=l):
+            vsend[l] = dot_nn(pick[l], v[...]).astype(BF16)
+            v_copies[l].start()
+
+    for i in range(2, 5):
+        settle(i)
+    dots = []
+    for c in head:
+        column = jnp.sum(og[:, c].astype(F32) * att[:, c].astype(F32), axis=1, keepdims=True)
+        dots.append(jnp.transpose(jnp.broadcast_to(column, (tok, 128)))[0:1, :])
+    stored = [log_sum[h : h + 1, :] for h in range(heads)]
+
+    def key_mask(chosen, r):
+        pieces = []
+        for m in live:
+            column = dot_nt(chosen, m.astype(BF16))[:, r : r + 1]
+            pieces.append(jnp.broadcast_to(column, (column.shape[0], QB)))
+        return jnp.concatenate(pieces, axis=1) > 0
+
+    own_mask = key_mask(jnp.where(below == above, 1.0, 0.0).astype(BF16), 0) & (below <= above)
+    for h, c in enumerate(head):
+        w = jnp.where(own_mask, jnp.exp(dot_nt(k[:, c], q[:, c]) * scale - stored[h]), 0.0)
+        dv_out[:, c] = dot_nn(w.astype(BF16), og[:, c])
+        g = (w * (dot_nt(v[:, c], og[:, c]) - dots[h])).astype(BF16)
+        dk_out[:, c] = dot_nn(g, q[:, c])
+        dq_out[:, c] = dot_tn(g, k[:, c])
+
+    masks = {
+        l: key_mask(one_hot(slot[l + 1 : l + 2, :]), l + 1) for l in order
+    }
+    load_x.wait()
+    width = x.shape[1] // CHUNKS
+    for i in range(CHUNKS):
+        xt[i * width : (i + 1) * width, :] = jnp.transpose(x[:, i * width : (i + 1) * width])
+    for l in order:
+
+        @pl.when(sends_down(l))
+        def _(l=l):
+            k_copies[l].wait_recv()
+            for h, c in enumerate(head):
+                w = jnp.where(
+                    masks[l], jnp.exp(dot_nt(kin[l, :, c], q[:, c]) * scale - stored[h]), 0.0
+                )
+                wts[l, h] = w
+                dvsend[l, :, c] = dot_nn(w.astype(BF16), og[:, c]).astype(BF16)
+            dv_copies[l].start()
+
+    for l in order:
+
+        @pl.when(sends_down(l))
+        def _(l=l):
+            v_copies[l].wait_recv()
+            for h, c in enumerate(head):
+                g = (wts[l, h] * (dot_nt(vin[l, :, c], og[:, c]) - dots[h])).astype(BF16)
+                dksend[l, :, c] = (dot_nn(g, q[:, c]) * scale).astype(BF16)
+                dq_out[:, c] += dot_tn(g, kin[l, :, c])
+            dk_copies[l].start()
+
     dq_out[...] = dq_out[...] * scale
 
-    total = dv_out[...]
-    for l in order:
-        dv_copies[l].wait_recv()
-        total += dot_tn(pick[l], dvin[l])
-    dv_out[...] = total
-    rounded = total.astype(BF16)
-    load_x.wait()
+    for l in order:
+
+        @pl.when(sends_up(l))
+        def _(l=l):
+            dv_copies[l].wait_recv()
+            dv_out[...] += dot_tn(pick[l], dvin[l])
+
+    rounded = dv_out[...].astype(BF16)
     core = lax.rem(me, 2)
     per = (n // 2) // CHUNKS
-    width = x.shape[1] // CHUNKS
     s1 = []
     for i in range(CHUNKS):
-        w = dot_tn(x[:, i * width : (i + 1) * width], rounded).reshape(per, 2, rb, cols)
+        w = dot_nn(xt[i * width : (i + 1) * width, :], rounded).reshape(per, 2, rb, cols)
         part[0, i * per : (i + 1) * per] = w[:, 0]
         part[1, i * per : (i + 1) * per] = w[:, 1]
         copy = remote(
@@ -218,18 +269,22 @@
             copy.start()
             s3.append(copy)
 
-    total = dk_out[...] * scale
-    for l in order:
-        dk_copies[l].wait_recv()
-        total += dot_tn(pick[l], dkin[l])
-    dk_out[...] = total
+    dk_out[...] = dk_out[...] * scale
+    for l in order:
+
+        @pl.when(sends_up(l))
+        def _(l=l):
+            dk_copies[l].wait_recv()
+            dk_out[...] += dot_tn(pick[l], dkin[l])
 
     for b, copy in zip(reversed(range(1, quarter)), s3):
         copy.wait_recv()
         wg_out[...] += got3[b].astype(F32)
-    for copies in (slot_copies, k_copies, v_copies, dv_copies, dk_copies):
-        for l in order:
-            copies[l].wait_send()
+    for l in order:
+        for copies in (slot_copies, dv_copies, dk_copies):
+            pl.when(sends_down(l))(copies[l].wait_send)
+        for copies in (k_copies, v_copies):
+            pl.when(sends_up(l))(copies[l].wait_send)
     for copy in s2 + s3:
         copy.wait_send()
 
@@ -242,7 +297,7 @@
     width = layer_input.shape[1]
     rb = width // n
     rows = (levels + 1 + 7) // 8 * 8
-    flat = [a.reshape(tok, cols) for a in (queries, keys, values, attended, out_grad)]
+    hbm = pl.BlockSpec(memory_space=pltpu.HBM)
     vmem = pl.BlockSpec(memory_space=pltpu.VMEM)
     sems = pltpu.SemaphoreType.DMA
     level_buf = pltpu.VMEM((levels, COMPACT, cols), BF16)
@@ -250,18 +305,23 @@
         functools.partial(body, n, levels, heads, dh),
         out_shape=[jax.ShapeDtypeStruct((tok, cols), F32)] * 3
         + [jax.ShapeDtypeStruct((rb, cols), F32)],
-        in_specs=[pl.BlockSpec(memory_space=pltpu.SMEM)] + [vmem] * 6
-        + [pl.BlockSpec(memory_space=pl.ANY)],
+        in_specs=[hbm] * 6 + [vmem, hbm],
         out_specs=[vmem] * 4,
         scratch_shapes=[
+            pltpu.SMEM(picked.shape, jnp.int32),
+            pltpu.VMEM((5, tok, heads, dh), BF16),
+        ]
+        + [pltpu.VMEM((tok, cols), BF16)] * 5
+        + [
             pltpu.VMEM((tok, width), BF16),
+            pltpu.VMEM((width, tok), BF16),
             pltpu.VMEM((rows, tok), F32),
             pltpu.VMEM((levels, rows, tok), F32),
             pltpu.VMEM((levels, COMPACT, tok), BF16),
         ]
         + [level_buf] * 8
         + [
-            pltpu.VMEM((levels, heads, tok, COMPACT), F32),
+            pltpu.VMEM((levels, heads, COMPACT, tok), F32),
             pltpu.VMEM((2, n // 2, rb, cols), F32),
             pltpu.VMEM((n // 2, rb, cols), F32),
             pltpu.VMEM((n // 4, rb, cols), BF16),
@@ -269,6 +329,8 @@
             pltpu.VMEM((n // 4, rb, cols), BF16),
             pltpu.VMEM((n // 4, rb, cols), BF16),
             sems,
+            sems,
+            sems((5,)),
         ]
         + [sems((levels,))] * 10
         + [sems((CHUNKS,))] * 2
@@ -276,7 +338,7 @@
         compiler_params=pltpu.CompilerParams(
             collective_id=0, has_side_effects=True, vmem_limit_bytes=48 * 1024 * 1024
         ),
-    )(picked, *flat, log_sum, layer_input)
+    )(picked, queries, keys, values, attended, out_grad, log_sum.T, layer_input)
     grads = [g.reshape(tok, heads, dh) for g in out[:3]]
     return (*grads, out[3])
 

time: 62.4 us -> 58 us (0.929)
  Pallas kernels: 52.3 us -> 46.4 us
  local copies, waits for them, and re-layouts: 9.21 us -> 10.7 us
    pallas_call x1, Pallas kernels: 52.3 us -> 46.4 us  [per_device(): pl.pallas_call(functools.partial(body, n, levels, heads, dh), out_shape=[...]
    unnamed x7 -> x17, local copies, waits for them, and re-layouts: 4.7 us -> 8.16 us
    reshape x2 -> x0, local copies, waits for them, and re-layouts: 2.01 us -> none  [per_device(): a.reshape(tok, cols)]
where the time goes in v1:
time: 58 us; the launch traced here: 57.8 us
  Pallas kernels  46.4 us (80%)
  local copies, waits for them, and re-layouts  10.7 us (18%)
  between operations  0.66 us (1%)
    pallas_call x1, Pallas kernels, per_device(): pl.pallas_call(functools.partial(body, n, levels, heads, dh), out_shape=[...  46.4 us
    unnamed x17, local copies, waits for them, and re-layouts  8.16 us
    reshape x3, local copies, waits for them, and re-layouts, per_device(): grads = [g.reshape(tok, heads, dh) for g in out[:3]]  2.5 us

profile of v1, /device:TPU:0, one launch (start us, length us, event | category | flops | bytes accessed | tf_op | source)
XLA Modules:
  0.0 57.8 jit_solution(11525614048050073511)
XLA Ops:
  0.6 0.0 copy-start
  0.6 1.6 %copy-done = bf16[256,4096]{1,0:T(8,128)(2,1)S(1)} copy-done((bf16[256,4096]{1,0:T(8,128)(2,1)S(1)}, bf16[256,4096]{1,0:T(8,128)(2,1)}, u32[]{:S(2)}) %copy-start) | copy-done | bytes 2097176
  2.2 0.0 copy-start.1
  2.2 0.9 %copy-done.1 = bf16[256,2,128]{2,1,0:T(2,128)(2,1)S(1)} copy-done((bf16[256,2,128]{2,1,0:T(2,128)(2,1)S(1)}, bf16[256,2,128]{2,1,0:T(2,128)(2,1)}, u32[]{:S(2)}) %copy-start.1) | copy-done | bytes 131096
  3.1 0.0 copy-start.2
  3.1 0.9 %copy-done.2 = bf16[256,2,128]{2,1,0:T(2,128)(2,1)S(1)} copy-done((bf16[256,2,128]{2,1,0:T(2,128)(2,1)S(1)}, bf16[256,2,128]{2,1,0:T(2,128)(2,1)}, u32[]{:S(2)}) %copy-start.2) | copy-done | bytes 131096
  4.0 0.0 copy-start.3
  4.0 0.9 %copy-done.3 = bf16[256,2,128]{2,1,0:T(2,128)(2,1)S(1)} copy-done((bf16[256,2,128]{2,1,0:T(2,128)(2,1)S(1)}, bf16[256,2,128]{2,1,0:T(2,128)(2,1)}, u32[]{:S(2)}) %copy-start.3) | copy-done | bytes 131096
  4.9 0.0 copy-start.4
  4.9 0.9 %copy-done.4 = bf16[256,2,128]{2,1,0:T(2,128)(2,1)S(1)} copy-done((bf16[256,2,128]{2,1,0:T(2,128)(2,1)S(1)}, bf16[256,2,128]{2,1,0:T(2,128)(2,1)}, u32[]{:S(2)}) %copy-start.4) | copy-done | bytes 131096
  5.8 0.0 copy-start.5
  5.8 0.9 %copy-done.5 = bf16[256,2,128]{2,1,0:T(2,128)(2,1)S(1)} copy-done((bf16[256,2,128]{2,1,0:T(2,128)(2,1)S(1)}, bf16[256,2,128]{2,1,0:T(2,128)(2,1)}, u32[]{:S(2)}) %copy-start.5) | copy-done | bytes 131096
  6.7 0.0 copy-start.6
  6.8 0.7 %copy-done.6 = f32[256,2]{0,1:T(2,128)S(1)} copy-done((f32[256,2]{0,1:T(2,128)S(1)}, f32[256,2]{0,1:T(2,128)}, u32[]{:S(2)}) %copy-start.6) | copy-done | bytes 2072
  7.4 0.0 copy-start.7
  7.4 0.7 %copy-done.7 = s32[2,16]{1,0:T(2,128)S(1)} copy-done((s32[2,16]{1,0:T(2,128)S(1)}, s32[2,16]{1,0:T(2,128)}, u32[]{:S(2)}) %copy-start.7) | copy-done | bytes 152
  8.1 46.4 %shard_map.111 = (f32[256,256]{1,0:T(8,128)S(1)}, f32[256,256]{1,0:T(8,128)S(1)}, f32[256,256]{1,0:T(8,128)S(1)}, f32[256,256]{1,0:T(8,128)S(1)}) custom-call(s32[2,16]{1,0:T(2,128)S(1)} %copy-done.7, bf16[256,2,128]{2,1,0:T(2,128)(2,1)S(1)} %copy-done.1, bf16[256,2,128]{2,1,0:T(2,128)(2,1)S(1)} %copy-done.2, bf16[256,2,128]{2,1,0:T(2,128)(2,1)S(1)} %copy-done.3, ...), custom_call_target="tpu_custom_call" | custom-call | tf_op jit(solution)/shard_map/pallas_call | solution.py:304
  54.6 0.8 %reshape.17 = f32[256,2,128]{2,1,0:T(2,128)} reshape(f32[256,256]{1,0:T(8,128)S(1)} %get-tuple-element.8) | data formatting | bytes 524288 | tf_op jit(solution)/shard_map/reshape | solution.py:342
  55.4 0.8 %reshape.18 = f32[256,2,128]{2,1,0:T(2,128)} reshape(f32[256,256]{1,0:T(8,128)S(1)} %get-tuple-element.9) | data formatting | bytes 524288 | tf_op jit(solution)/shard_map/reshape | solution.py:342
  56.2 0.8 %reshape.19 = f32[256,2,128]{2,1,0:T(2,128)} reshape(f32[256,256]{1,0:T(8,128)S(1)} %get-tuple-element.10) | data formatting | bytes 524288 | tf_op jit(solution)/shard_map/reshape | solution.py:342
  57.1 0.7 %copy.13 = f32[256,256]{1,0:T(8,128)} copy(f32[256,256]{1,0:T(8,128)S(1)} %get-tuple-element.19) | data formatting | bytes 524288
Async XLA Ops:
  0.6 1.6 %copy-start = (bf16[256,4096]{1,0:T(8,128)(2,1)S(1)}, bf16[256,4096]{1,0:T(8,128)(2,1)}, u32[]{:S(2)}) copy-start(bf16[256,4096]{1,0:T(8,128)(2,1)} %x_hbm.1) | copy-start | bytes 6291460
  2.2 0.9 %copy-start.1 = (bf16[256,2,128]{2,1,0:T(2,128)(2,1)S(1)}, bf16[256,2,128]{2,1,0:T(2,128)(2,1)}, u32[]{:S(2)}) copy-start(bf16[256,2,128]{2,1,0:T(2,128)(2,1)} %q_hbm.1) | copy-start | bytes 393220
  3.1 0.9 %copy-start.2 = (bf16[256,2,128]{2,1,0:T(2,128)(2,1)S(1)}, bf16[256,2,128]{2,1,0:T(2,128)(2,1)}, u32[]{:S(2)}) copy-start(bf16[256,2,128]{2,1,0:T(2,128)(2,1)} %k_hbm.1) | copy-start | bytes 393220
  4.0 0.9 %copy-start.3 = (bf16[256,2,128]{2,1,0:T(2,128)(2,1)S(1)}, bf16[256,2,128]{2,1,0:T(2,128)(2,1)}, u32[]{:S(2)}) copy-start(bf16[256,2,128]{2,1,0:T(2,128)(2,1)} %v_hbm.1) | copy-start | bytes 393220
  4.9 0.9 %copy-start.4 = (bf16[256,2,128]{2,1,0:T(2,128)(2,1)S(1)}, bf16[256,2,128]{2,1,0:T(2,128)(2,1)}, u32[]{:S(2)}) copy-start(bf16[256,2,128]{2,1,0:T(2,128)(2,1)} %att_hbm.1) | copy-start | bytes 393220
  5.8 0.9 %copy-start.5 = (bf16[256,2,128]{2,1,0:T(2,128)(2,1)S(1)}, bf16[256,2,128]{2,1,0:T(2,128)(2,1)}, u32[]{:S(2)}) copy-start(bf16[256,2,128]{2,1,0:T(2,128)(2,1)} %og_hbm.1) | copy-start | bytes 393220
  6.7 0.7 %copy-start.6 = (f32[256,2]{0,1:T(2,128)S(1)}, f32[256,2]{0,1:T(2,128)}, u32[]{:S(2)}) copy-start(f32[256,2]{0,1:T(2,128)} %param.13) | copy-start | bytes 6148
  7.4 0.7 %copy-start.7 = (s32[2,16]{1,0:T(2,128)S(1)}, s32[2,16]{1,0:T(2,128)}, u32[]{:S(2)}) copy-start(s32[2,16]{1,0:T(2,128)} %picked_hbm.1) | copy-start | bytes 388

commit v2 on v1

--- a/solution.py
+++ b/solution.py
@@ -198,7 +198,7 @@
     width = x.shape[1] // CHUNKS
     for i in range(CHUNKS):
         xt[i * width : (i + 1) * width, :] = jnp.transpose(x[:, i * width : (i + 1) * width])
-    for l in order:
+    for l in range(levels):
 
         @pl.when(sends_down(l))
         def _(l=l):
@@ -211,7 +211,7 @@
                 dvsend[l, :, c] = dot_nn(w.astype(BF16), og[:, c]).astype(BF16)
             dv_copies[l].start()
 
-    for l in order:
+    for l in range(levels):
 
         @pl.when(sends_down(l))
         def _(l=l):
@@ -224,7 +224,7 @@
 
     dq_out[...] = dq_out[...] * scale
 
-    for l in order:
+    for l in range(levels):
 
         @pl.when(sends_up(l))
         def _(l=l):
@@ -233,33 +233,35 @@
 
     rounded = dv_out[...].astype(BF16)
     core = lax.rem(me, 2)
-    per = (n // 2) // CHUNKS
-    s1 = []
-    for i in range(CHUNKS):
-        w = dot_nn(xt[i * width : (i + 1) * width, :], rounded).reshape(per, 2, rb, cols)
-        part[0, i * per : (i + 1) * per] = w[:, 0]
-        part[1, i * per : (i + 1) * per] = w[:, 1]
+    up = lax.rem(me, 4) // 2
+    high = me // 4
+    far = list(reversed(range(quarter)))
+    chunk = 2 * rb
+    s1, s2, s3 = [], [], []
+
+    def share(t, at):
+        first = pl.multiple_of(at * chunk, chunk)
+        w = dot_nn(xt[pl.ds(first, chunk), :], rounded)
+        part[t] = w.reshape(2, rb, cols)
         copy = remote(
-            part.at[1 - core, pl.ds(i * per, per)], got1.at[pl.ds(i * per, per)],
-            s1_ss.at[i], s1_rs.at[i], flipped(1),
+            part.at[t, 1 - core], got1.at[t], s1_ss.at[t], s1_rs.at[t], flipped(1)
         )
         copy.start()
         s1.append(copy)
-    for copy in s1:
-        copy.wait()
-    up = lax.rem(me, 4) // 2
-    high = me // 4
-    s2, s3 = [], []
-    for b in reversed(range(quarter)):
-        at = 2 * xor(high, b) + 1 - up
-        send2[b] = (part[core, at] + got1[at]).astype(BF16)
+
+    for t, b in enumerate(far):
+        share(t, 2 * xor(high, b) + 1 - up)
+    for t, b in enumerate(far):
+        share(quarter + t, 2 * xor(high, b) + up)
+        s1[t].wait_recv()
+        send2[b] = (part[t, core] + got1[t]).astype(BF16)
         copy = remote(send2.at[b], got2.at[b], s2_ss.at[b], s2_rs.at[b], flipped(2))
         copy.start()
         s2.append(copy)
-    for b, copy in zip(reversed(range(quarter)), s2):
-        at = 2 * xor(high, b) + up
-        kept = part[core, at] + got1[at]
-        copy.wait_recv()
+    for t, b in enumerate(far):
+        s1[quarter + t].wait_recv()
+        kept = part[quarter + t, core] + got1[quarter + t]
+        s2[t].wait_recv()
         kept = kept + got2[b].astype(F32)
         if b == 0:
             wg_out[...] = kept
@@ -270,7 +272,7 @@
             s3.append(copy)
 
     dk_out[...] = dk_out[...] * scale
-    for l in order:
+    for l in range(levels):
 
         @pl.when(sends_up(l))
         def _(l=l):
@@ -285,7 +287,7 @@
             pl.when(sends_down(l))(copies[l].wait_send)
         for copies in (k_copies, v_copies):
             pl.when(sends_up(l))(copies[l].wait_send)
-    for copy in s2 + s3:
+    for copy in s1 + s2 + s3:
         copy.wait_send()
 
 
@@ -322,7 +324,7 @@
         + [level_buf] * 8
         + [
             pltpu.VMEM((levels, heads, COMPACT, tok), F32),
-            pltpu.VMEM((2, n // 2, rb, cols), F32),
+            pltpu.VMEM((n // 2, 2, rb, cols), F32),
             pltpu.VMEM((n // 2, rb, cols), F32),
             pltpu.VMEM((n // 4, rb, cols), BF16),
             pltpu.VMEM((n // 4, rb, cols), BF16),
@@ -333,10 +335,10 @@
             sems((5,)),
         ]
         + [sems((levels,))] * 10
-        + [sems((CHUNKS,))] * 2
+        + [sems((n // 2,))] * 2
         + [sems((n // 4,))] * 4,
         compiler_params=pltpu.CompilerParams(
-            collective_id=0, has_side_effects=True, vmem_limit_bytes=48 * 1024 * 1024
+            collective_id=0, has_side_effects=True
         ),
     )(picked, queries, keys, values, attended, out_grad, log_sum.T, layer_input)
     grads = [g.reshape(tok, heads, dh) for g in out[:3]]

time: 58 us -> 54 us (0.931)
  local copies, waits for them, and re-layouts: 10.7 us -> 7.01 us
    unnamed x17 -> x1, local copies, waits for them, and re-layouts: 8.16 us -> 1.67 us
    reshape x3, local copies, waits for them, and re-layouts: 2.5 us -> 5.34 us  [per_device(): grads = [g.reshape(tok, heads, dh) for g in out[:3]]]
where the time goes in v2:
time: 54 us; the launch traced here: 53.7 us
  Pallas kernels  46.1 us (85%)
  local copies, waits for them, and re-layouts  7.01 us (13%)
  between operations  0.64 us (1%)
    pallas_call x1, Pallas kernels, per_device(): pl.pallas_call(functools.partial(body, n, levels, heads, dh), out_shape=[...  46.1 us
    reshape x3, local copies, waits for them, and re-layouts, per_device(): grads = [g.reshape(tok, heads, dh) for g in out[:3]]  5.34 us
    unnamed x1, local copies, waits for them, and re-layouts  1.67 us

profile of v2, /device:TPU:0, one launch (start us, length us, event | category | flops | bytes accessed | tf_op | source)
XLA Modules:
  0.0 53.7 jit_solution(17318599419691612370)
XLA Ops:
  0.6 46.1 %shard_map.111 = (f32[256,256]{1,0:T(8,128)}, f32[256,256]{1,0:T(8,128)}, f32[256,256]{1,0:T(8,128)}, f32[256,256]{1,0:T(8,128)}) custom-call(s32[2,16]{1,0:T(2,128)} %picked_hbm.1, bf16[256,2,128]{2,1,0:T(2,128)(2,1)} %q_hbm.1, bf16[256,2,128]{2,1,0:T(2,128)(2,1)} %k_hbm.1, bf16[256,2,128]{2,1,0:T(2,128)(2,1)} %v_hbm.1, bf16[256,2,128]{2,1,0:T(2,128)(2,1)} %att_hbm.1, ...), custom_call_target="tpu_custom_call" | custom-call | tf_op jit(solution)/shard_map/pallas_call | solution.py:306
  46.7 1.8 %reshape.17 = f32[256,2,128]{2,1,0:T(2,128)} reshape(f32[256,256]{1,0:T(8,128)} %get-tuple-element.8) | data formatting | bytes 524288 | tf_op jit(solution)/shard_map/reshape | solution.py:344
  48.5 1.8 %reshape.18 = f32[256,2,128]{2,1,0:T(2,128)} reshape(f32[256,256]{1,0:T(8,128)} %get-tuple-element.9) | data formatting | bytes 524288 | tf_op jit(solution)/shard_map/reshape | solution.py:344
  50.3 1.8 %reshape.19 = f32[256,2,128]{2,1,0:T(2,128)} reshape(f32[256,256]{1,0:T(8,128)} %get-tuple-element.10) | data formatting | bytes 524288 | tf_op jit(solution)/shard_map/reshape | solution.py:344
  52.0 1.7 %copy.13 = f32[256,256]{1,0:T(8,128)} copy(f32[256,256]{1,0:T(8,128)} %get-tuple-element.19) | data formatting | bytes 524288

commit v3 on v2

--- a/solution.py
+++ b/solution.py
@@ -289,6 +289,14 @@
             pl.when(sends_up(l))(copies[l].wait_send)
     for copy in s1 + s2 + s3:
         copy.wait_send()
+
+
+def finish(dq, dk, dv, wg, dq_out, dk_out, dv_out, wg_out):
+    heads, dh = dq_out.shape[1:]
+    for src, dst in ((dq, dq_out), (dk, dk_out), (dv, dv_out)):
+        for h in range(heads):
+            dst[:, h, :] = src[:, h * dh : (h + 1) * dh]
+    wg_out[...] = wg[...]
 
 
 def per_device(queries, keys, values, attended, out_grad, log_sum, picked, layer_input):
@@ -341,8 +349,13 @@
             collective_id=0, has_side_effects=True
         ),
     )(picked, queries, keys, values, attended, out_grad, log_sum.T, layer_input)
-    grads = [g.reshape(tok, heads, dh) for g in out[:3]]
-    return (*grads, out[3])
+    return pl.pallas_call(
+        finish,
+        out_shape=[jax.ShapeDtypeStruct((tok, heads, dh), F32)] * 3
+        + [jax.ShapeDtypeStruct((rb, cols), F32)],
+        in_specs=[vmem] * 4,
+        out_specs=[vmem] * 4,
+    )(*out)
 
 
 def solution(mesh):

time: 54 us -> 49.2 us (0.911)
  local copies, waits for them, and re-layouts: 7.01 us -> 0 us
  Pallas kernels: 46.1 us -> 48.4 us
    reshape x3 -> x0, local copies, waits for them, and re-layouts: 5.34 us -> none  [per_device(): grads = [g.reshape(tok, heads, dh) for g in out[:3]]]
    pallas_call x0 -> x1, Pallas kernels: none -> 2.36 us  [per_device(): pl.pallas_call(finish, out_shape=[jax.ShapeDtypeStruct((tok, heads, dh),...]
    unnamed x1 -> x0, local copies, waits for them, and re-layouts: 1.67 us -> none
where the time goes in v3:
time: 49.2 us; the launch traced here: 49.1 us
  Pallas kernels  48.4 us (98%)
  between operations  0.64 us (1%)
    pallas_call x1, Pallas kernels, per_device(): pl.pallas_call(functools.partial(body, n, levels, heads, dh), out_shape=[...  46.1 us
    pallas_call x1, Pallas kernels, per_device(): pl.pallas_call(finish, out_shape=[jax.ShapeDtypeStruct((tok, heads, dh),...  2.36 us

profile of v3, /device:TPU:0, one launch (start us, length us, event | category | flops | bytes accessed | tf_op | source)
XLA Modules:
  0.0 49.1 jit_solution(13936607730364542260)
XLA Ops:
  0.6 46.1 %shard_map.111 = (f32[256,256]{1,0:T(8,128)}, f32[256,256]{1,0:T(8,128)}, f32[256,256]{1,0:T(8,128)}, f32[256,256]{1,0:T(8,128)}) custom-call(s32[2,16]{1,0:T(2,128)} %picked_hbm.1, bf16[256,2,128]{2,1,0:T(2,128)(2,1)} %q_hbm.1, bf16[256,2,128]{2,1,0:T(2,128)(2,1)} %k_hbm.1, bf16[256,2,128]{2,1,0:T(2,128)(2,1)} %v_hbm.1, bf16[256,2,128]{2,1,0:T(2,128)(2,1)} %att_hbm.1, ...), custom_call_target="tpu_custom_call" | custom-call | tf_op jit(solution)/shard_map/pallas_call | solution.py:314
  46.7 2.4 %shard_map.112 = (f32[256,2,128]{2,1,0:T(2,128)}, f32[256,2,128]{2,1,0:T(2,128)}, f32[256,2,128]{2,1,0:T(2,128)}, f32[256,256]{1,0:T(8,128)}) custom-call(f32[256,256]{1,0:T(8,128)} %get-tuple-element.8.dq, f32[256,256]{1,0:T(8,128)} %get-tuple-element.9.dk, f32[256,256]{1,0:T(8,128)} %get-tuple-element.10.dv, f32[256,256]{1,0:T(8,128)} %get-tuple-element.11.wg), custom_call_target="tpu_custom_call" | custom-call | tf_op jit(solution)/shard_map/pallas_call | solution.py:352
